TPU v7x, 32 devices: a whole 2x2x4 slice. The times are simulated.
32 devices in a mesh: grp: 1, sp: 8 (over z, core), tp: 4 (over y, x).
Axes of the slice: x: 2, y: 2, z: 4, core: 2. Of those that a mesh axis runs over, the one named last changes fastest.
Arguments:
- queries: bfloat16 [2048, 16, 128], P(('grp', 'sp'), 'tp'), may hold values from -6 to 6
- keys: bfloat16 [2048, 4, 128], P(('grp', 'sp'), 'tp'), may hold values from -6 to 6
- values: bfloat16 [2048, 4, 128], P(('grp', 'sp'), 'tp'), may hold values from -6 to 6
- log_gates: float32 [16, 2048], P('tp', ('grp', 'sp')), may hold values from -260 to 0, as said below
- documents: int32 [2048], P(('grp', 'sp')), may hold values from 0 to 2, never falling along the last dimension, each value on 1 to 1536 neighbouring positions
- query_gain: float32 [128], replicated, may hold values from 0.5 to 5
- key_gain: float32 [128], replicated, may hold values from 0.5 to 5
- out_weight: bfloat16 [2048, 2048], P('tp'), may hold values from -0.125 to 0.125
- residual: bfloat16 [2048, 2048], P(('grp', 'sp', 'tp')), may hold values from -1.5 to 1.5
- norm_gain: float32 [2048], replicated, may hold values from 0.1 to 1.9
- routes: int32 [2048, 2], P(('grp', 'sp', 'tp')), may hold values from 0 to 3, all different within a row; in each aligned block of 64 rows (0 to 63, 64 to 127, ...) at most 48 rows name the same one
- route_weights: float32 [2048, 2], P(('grp', 'sp', 'tp')), may hold values from 0.1 to 1
- w_gate: bfloat16 [8, 2048, 2048], P('sp', None, 'tp'), may hold values from -0.125 to 0.125
- w_up: bfloat16 [8, 2048, 2048], P('sp', None, 'tp'), may hold values from -0.125 to 0.125
- w_down: bfloat16 [8, 2048, 2048], P('sp', 'tp'), may hold values from -0.09375 to 0.09375
Outputs:
- layer_out: bfloat16 [2048, 2048], P(('grp', 'sp', 'tp'))
Inputs may be any that keep to these rules, and one draw needn't show every extreme that they name: `log_gates`: non-increasing along positions for every head. `documents`: never falls along positions. `routes`: the 2 experts of a token differ; among the 64 tokens of one device (aligned blocks) no expert is named by more than 48 tokens, and in every draw some expert is named by exactly 48 of them.
All inputs are finite; a program needn't handle non-finite values.
Results may differ from a plain program's by a relative error of at most 0.017.
The roundings to bfloat16 on the way count: a program that leaves them out, or rounds other values in their place, can miss the bound.
Values may be sent and summed in bfloat16 or wider, within the bound.
A program may use at most 128 MiB of HBM per device.

v0:
```python
import functools

import jax
import jax.numpy as jnp
from jax import lax
from jax.experimental import pallas as pl
from jax.experimental.pallas import tpu as pltpu
from jax.sharding import PartitionSpec as P

EPSILON = 1e-06
CHUNK = 16
MESH = pl.DeviceIdType.MESH


def rms_scale(inputs, gain):
    return inputs * lax.rsqrt(jnp.mean(inputs * inputs, axis=-1, keepdims=True) + EPSILON) * gain


def flip(index, bits):
    index = index + (bits % 2) * (1 - 2 * (index % 2))
    return index + (bits // 2) * (2 - 4 * ((index // 2) % 2))


def greet(nz, n_tp, z, c, t):
    barrier = pltpu.get_barrier_semaphore()
    for dz in range(1, nz):
        pl.semaphore_signal(
            barrier, inc=1, device_id={"sp": 2 * ((z + dz) % nz) + c}, device_id_type=MESH
        )
    for k in range(1, n_tp):
        pl.semaphore_signal(barrier, inc=1, device_id={"tp": flip(t, k)}, device_id_type=MESH)
    pl.semaphore_signal(barrier, inc=1, device_id={"sp": 2 * z + 1 - c}, device_id_type=MESH)
    pl.semaphore_wait(barrier, nz - 1 + n_tp - 1 + 1)


def attend_kernel(
    nz,
    n_tp,
    q_ref,
    kv_ref,
    gd_ref,
    col_ref,
    w_ref,
    res_ref,
    gain_ref,
    mixed_ref,
    normed_ref,
    kv_buf,
    gd_buf,
    m_ref,
    l_ref,
    acc_ref,
    att_ref,
    sbuf,
    rbuf,
    kv_send,
    kv_recv,
    gd_send,
    gd_recv,
    fkv_send,
    fgd_send,
    rs_send,
    rs_recv,
):
    s = lax.axis_index("sp")
    t = lax.axis_index("tp")
    z, c = s // 2, s % 2
    heads, rows, hd = q_ref.shape
    greet(nz, n_tp, z, c, t)

    def own_copies(slot, target):
        return (
            pltpu.make_async_remote_copy(
                kv_ref, kv_buf.at[s], kv_send.at[slot], kv_recv.at[s],
                device_id={"sp": target}, device_id_type=MESH,
            ),
            pltpu.make_async_remote_copy(
                gd_ref, gd_buf.at[s], gd_send.at[slot], gd_recv.at[s],
                device_id={"sp": target}, device_id_type=MESH,
            ),
        )

    def fwd_copies(source, slot):
        return (
            pltpu.make_async_remote_copy(
                kv_buf.at[source], kv_buf.at[source], fkv_send.at[slot], kv_recv.at[source],
                device_id={"sp": 2 * z + 1 - c}, device_id_type=MESH,
            ),
            pltpu.make_async_remote_copy(
                gd_buf.at[source], gd_buf.at[source], fgd_send.at[slot], gd_recv.at[source],
                device_id={"sp": 2 * z + 1 - c}, device_id_type=MESH,
            ),
        )

    def begin(dz, carry):
        for copy in own_copies(dz, 2 * (z + dz) + c):
            copy.start()
        return carry

    @pl.when(c == 0)
    def _():
        for copy in own_copies(0, 2 * z + 1):
            copy.start()

    lax.fori_loop(1, nz - z, begin, 0)

    def update(keys, values, gates, docs, causal, first):
        same = docs == col_ref[:, heads:heads + 1]
        if causal:
            qi = lax.broadcasted_iota(jnp.int32, (rows, rows), 0)
            ki = lax.broadcasted_iota(jnp.int32, (rows, rows), 1)
            same = same & (ki <= qi)
        for h in range(heads):
            scores = lax.dot_general(
                q_ref[h], keys, (((1,), (1,)), ((), ())), preferred_element_type=jnp.float32
            )
            scores = scores + col_ref[:, h:h + 1] - gates[h:h + 1, :]
            scores = jnp.where(same, scores, -jnp.inf)
            peak = jnp.max(scores, axis=-1, keepdims=True)
            if first:
                expo = jnp.exp(scores - peak)
                l_ref[h] = jnp.sum(expo, axis=-1, keepdims=True)
                m_ref[h] = peak
                acc_ref[h] = jnp.dot(
                    expo.astype(jnp.bfloat16), values, preferred_element_type=jnp.float32
                )
            else:
                old = m_ref[h]
                new = jnp.maximum(old, peak)
                expo = jnp.exp(scores - new)
                factor = jnp.exp(old - new)
                l_ref[h] = factor * l_ref[h] + jnp.sum(expo, axis=-1, keepdims=True)
                m_ref[h] = new
                acc_ref[h] = factor * acc_ref[h] + jnp.dot(
                    expo.astype(jnp.bfloat16), values, preferred_element_type=jnp.float32
                )

    update(
        kv_ref[:, :hd], kv_ref[:, hd:], gd_ref[...], gd_ref[heads:heads + 1, :], True, True
    )

    def take(source):
        update(
            kv_buf[source, :, :hd],
            kv_buf[source, :, hd:],
            gd_buf[source],
            gd_buf[source, heads:heads + 1, :],
            False,
            False,
        )

    def one_source(i, carry):
        dz = (i + 1) // 2
        direct = i % 2
        core = (1 - direct) * (1 - c) + direct * c
        source = 2 * (z - dz) + core
        for copy in fwd_copies(source, dz):
            copy.wait_recv()

        @pl.when(direct == 1)
        def _():
            for copy in fwd_copies(source, dz):
                copy.start()

        take(source)
        return carry

    lax.fori_loop(1 - c, 2 * z + 1, one_source, 0)

    for h in range(heads):
        att_ref[:, h * hd:(h + 1) * hd] = (acc_ref[h] / l_ref[h]).astype(jnp.bfloat16)

    share = rows // n_tp

    def project(i, carry):
        k = n_tp - 1 - i
        start = pl.multiple_of(flip(t, k) * share, share)
        block = jnp.dot(
            att_ref[pl.ds(start, share), :], w_ref[...], preferred_element_type=jnp.float32
        )
        sbuf[k] = block.astype(jnp.bfloat16)

        @pl.when(k > 0)
        def _():
            pltpu.make_async_remote_copy(
                sbuf.at[k], rbuf.at[k], rs_send.at[k], rs_recv.at[k],
                device_id={"tp": flip(t, k)}, device_id_type=MESH,
            ).start()

        return carry

    lax.fori_loop(0, n_tp, project, 0)

    for k in range(1, n_tp):
        copy = pltpu.make_async_remote_copy(
            sbuf.at[k], rbuf.at[k], rs_send.at[k], rs_recv.at[k],
            device_id={"tp": flip(t, k)}, device_id_type=MESH,
        )
        copy.wait_recv()

    def finish(i, carry):
        part = pl.ds(pl.multiple_of(i * CHUNK, CHUNK), CHUNK)
        total = sbuf[0, part, :].astype(jnp.float32)
        for k in range(1, n_tp):
            total = total + rbuf[k, part, :].astype(jnp.float32)
        mixed = (res_ref[part, :].astype(jnp.float32) + total).astype(jnp.bfloat16)
        mixed_ref[part, :] = mixed
        normed_ref[part, :] = rms_scale(mixed.astype(jnp.float32), gain_ref[...]).astype(
            jnp.bfloat16
        )
        return carry

    lax.fori_loop(0, share // CHUNK, finish, 0)

    for k in range(1, n_tp):
        pltpu.make_async_remote_copy(
            sbuf.at[k], rbuf.at[k], rs_send.at[k], rs_recv.at[k],
            device_id={"tp": flip(t, k)}, device_id_type=MESH,
        ).wait_send()

    def end(dz, carry):
        for copy in own_copies(dz, 2 * (z + dz) + c):
            copy.wait_send()
        return carry

    @pl.when(c == 0)
    def _():
        for copy in own_copies(0, 2 * z + 1):
            copy.wait_send()

    lax.fori_loop(1, nz - z, end, 0)

    def end_forward(dz, carry):
        for copy in fwd_copies(2 * (z - dz) + c, dz):
            copy.wait_send()
        return carry

    lax.fori_loop(1, z + 1, end_forward, 0)


def expert_kernel(
    nz,
    n_tp,
    out_ref,
    wg_hbm,
    wu_hbm,
    wd_hbm,
    ret_ref,
    wg_ref,
    wu_ref,
    wd_ref,
    arrived,
    part,
    pbuf,
    rbuf,
    hbuf,
    fin,
    w_sem,
    a_send,
    a_recv,
    b_send,
    b_recv,
    f_send,
    f_recv,
    d_send,
    d_recv,
    p_send,
    p_recv,
    h_send,
    h_recv,
    r_send,
    r_recv,
    z_send,
    z_recv,
):
    s = lax.axis_index("sp")
    t = lax.axis_index("tp")
    z, c = s // 2, s % 2
    _, cap, width = out_ref.shape
    rows = 2 * n_tp * cap
    partner = {"sp": 2 * z + 1 - c}
    near = 1 + c
    far = 2 - c

    loads = [
        pltpu.make_async_copy(src, dst, w_sem.at[i])
        for i, (src, dst) in enumerate(((wg_hbm, wg_ref), (wu_hbm, wu_ref), (wd_hbm, wd_ref)))
    ]
    for load in loads:
        load.start()
    greet(nz, n_tp, z, c, t)

    def remote(src, dst, send, recv, where):
        return pltpu.make_async_remote_copy(
            src, dst, send, recv, device_id=where, device_id_type=MESH
        )

    def source_of(q):
        return (z + nz - q) % nz

    def mine(q):
        return arrived.at[source_of(q), c, t]

    def along(q):
        target = (z + q) % nz
        return remote(
            out_ref.at[target], arrived.at[z, c, t], a_send.at[q], a_recv.at[q],
            {"sp": 2 * target + c},
        )

    def along_in(q):
        return remote(mine(q), mine(q), a_send.at[q], a_recv.at[q], partner)

    def spread(q, k, src):
        where = {"tp": flip(t, k)} if k else partner
        return remote(src, mine(q), b_send.at[k, q], b_recv.at[k, q], where)

    def spread_in(q, k):
        block = arrived.at[source_of(q), c, flip(t, k)] if k else arrived.at[
            source_of(q), 1 - c, t
        ]
        return remote(block, block, b_send.at[k, q], b_recv.at[k, q], partner)

    def diagonal(q):
        block = arrived.at[source_of(q), c, flip(t, far)]
        return remote(block, block, f_send.at[q], f_recv.at[q], {"tp": flip(t, near)})

    def diagonal_in(q):
        block = arrived.at[source_of(q), c, flip(t, 3)]
        return remote(block, block, f_send.at[q], f_recv.at[q], partner)

    def to_partner(q, k):
        block = arrived.at[source_of(q), c, flip(t, k)]
        return remote(block, block, d_send.at[k, q], d_recv.at[k, q], partner)

    def from_partner(q, k):
        block = arrived.at[source_of(q), 1 - c, flip(t, k)]
        return remote(block, block, d_send.at[k, q], d_recv.at[k, q], partner)

    def part_out(q):
        return remote(part.at[q, 1 - c], pbuf.at[q], p_send.at[q], p_recv.at[q], partner)

    def hand_over(q):
        return remote(
            part.at[q, c, flip(t, 3)], hbuf.at[q], h_send.at[q], h_recv.at[q],
            {"tp": flip(t, near)},
        )

    def reduce_near(q):
        return remote(
            part.at[q, c, flip(t, near)], rbuf.at[q, 0], r_send.at[0, q], r_recv.at[0, q],
            {"tp": flip(t, near)},
        )

    def reduce_far(q):
        return remote(
            part.at[q, c, flip(t, far)], rbuf.at[q, 1], r_send.at[1, q], r_recv.at[1, q],
            {"tp": flip(t, far)},
        )

    def home(q):
        return remote(
            fin.at[q], ret_ref.at[z], z_send.at[q], z_recv.at[q], {"sp": 2 * source_of(q) + c}
        )

    def home_in(q):
        return remote(
            fin.at[q], ret_ref.at[(z + q) % nz], z_send.at[q], z_recv.at[q], partner
        )

    for k in (1, 2, 0):
        spread(0, k, out_ref.at[z]).start()

    def begin(q, carry):
        along(q).start()
        return carry

    lax.fori_loop(1, nz, begin, 0)
    arrived[z, c, t] = out_ref[z]
    for load in loads:
        load.wait()

    def add_pair(q, column):
        def one(r, carry):
            at = pl.ds(pl.multiple_of(r * CHUNK, CHUNK), CHUNK)
            total = part[q, c, column, at, :].astype(jnp.float32) + pbuf[
                q, column, at, :
            ].astype(jnp.float32)
            part[q, c, column, at, :] = total.astype(jnp.bfloat16)
            return carry

        lax.fori_loop(0, cap // CHUNK, one, 0)

    def step(i, carry):
        p = i - 1

        @pl.when(p + 2 < nz)
        def _():
            q = p + 2
            along_in(q).wait_recv()
            for k in (1, 2, 0):
                spread(q, k, mine(q)).start()

        @pl.when(p + 1 < nz)
        def _():
            q = p + 1
            spread_in(q, 1).wait_recv()
            to_partner(q, 1).start()
            spread_in(q, 2).wait_recv()
            diagonal(q).start()
            to_partner(q, 2).start()
            spread_in(q, 0).wait_recv()

        @pl.when((p >= 0) & (p < nz))
        def _():
            diagonal_in(p).wait_recv()
            to_partner(p, 3).start()
            for k in range(1, n_tp):
                from_partner(p, k).wait_recv()
            flat = arrived[source_of(p)].reshape(rows, width)
            gate = jnp.dot(flat, wg_ref[...], preferred_element_type=jnp.float32)
            up = jnp.dot(flat, wu_ref[...], preferred_element_type=jnp.float32)
            hidden = (gate * (1.0 / (1.0 + jnp.exp(-gate))) * up).astype(jnp.bfloat16)
            result = jnp.dot(hidden, wd_ref[...], preferred_element_type=jnp.float32)
            part[p] = result.astype(jnp.bfloat16).reshape(2, n_tp, cap, width)
            part_out(p).start()

        @pl.when((p >= 1) & (p - 1 < nz))
        def _():
            q = p - 1
            part_out(q).wait_recv()
            add_pair(q, flip(t, 3))
            hand_over(q).start()
            add_pair(q, flip(t, near))
            reduce_near(q).start()
            add_pair(q, flip(t, far))
            add_pair(q, t)

        @pl.when((p >= 2) & (p - 2 < nz))
        def _():
            q = p - 2
            column = flip(t, far)
            hand_over(q).wait_recv()

            def one(r, carry):
                at = pl.ds(pl.multiple_of(r * CHUNK, CHUNK), CHUNK)
                total = part[q, c, column, at, :].astype(jnp.float32) + hbuf[q, at, :].astype(
                    jnp.float32
                )
                part[q, c, column, at, :] = total.astype(jnp.bfloat16)
                return carry

            lax.fori_loop(0, cap // CHUNK, one, 0)
            reduce_far(q).start()

        @pl.when(p >= 3)
        def _():
            q = p - 3
            reduce_near(q).wait_recv()
            reduce_far(q).wait_recv()

            def one(r, carry):
                at = pl.ds(pl.multiple_of(r * CHUNK, CHUNK), CHUNK)
                total = (
                    part[q, c, t, at, :].astype(jnp.float32)
                    + rbuf[q, 0, at, :].astype(jnp.float32)
                    + rbuf[q, 1, at, :].astype(jnp.float32)
                )
                fin[q, at, :] = total.astype(jnp.bfloat16)
                return carry

            lax.fori_loop(0, cap // CHUNK, one, 0)

            @pl.when(q > 0)
            def _():
                home(q).start()

            @pl.when(q == 0)
            def _():
                ret_ref[z] = fin[0]

        return carry

    lax.fori_loop(0, nz + 4, step, 0)

    def drain(q, carry):
        home_in(q).wait_recv()
        home(q).wait_send()
        along(q).wait_send()
        return carry

    lax.fori_loop(1, nz, drain, 0)

    def drain_plane(q, carry):
        for k in range(3):
            spread(q, k, mine(q)).wait_send()
        diagonal(q).wait_send()
        for k in range(1, n_tp):
            to_partner(q, k).wait_send()
        part_out(q).wait_send()
        hand_over(q).wait_send()
        reduce_near(q).wait_send()
        reduce_far(q).wait_send()
        return carry

    lax.fori_loop(0, nz, drain_plane, 0)


def local(
    nz,
    n_tp,
    queries,
    keys,
    values,
    log_gates,
    documents,
    query_gain,
    key_gain,
    out_weight,
    residual,
    norm_gain,
    routes,
    route_weights,
    w_gate,
    w_up,
    w_down,
):
    tok_dev, heads, head_size = queries.shape
    model_dim = residual.shape[1]
    rows_dev = tok_dev // n_tp
    n_sp = 2 * nz
    query_norm = (rms_scale(queries.astype(jnp.float32), query_gain) * head_size ** (-0.5)).astype(
        jnp.bfloat16
    )
    key_norm = rms_scale(keys[:, 0, :].astype(jnp.float32), key_gain).astype(jnp.bfloat16)
    kv = jnp.concatenate([key_norm, values[:, 0, :]], axis=1)
    pad = (-(heads + 1)) % 8
    gates_docs = jnp.concatenate(
        [
            log_gates,
            documents.astype(jnp.float32)[None, :],
            jnp.zeros((pad, tok_dev), jnp.float32),
        ],
        axis=0,
    )
    vmem = pl.BlockSpec(memory_space=pltpu.VMEM)
    hbm = pl.BlockSpec(memory_space=pl.ANY)
    dma = pltpu.SemaphoreType.DMA
    mixed, normed = pl.pallas_call(
        functools.partial(attend_kernel, nz, n_tp),
        out_shape=(
            jax.ShapeDtypeStruct((rows_dev, model_dim), jnp.bfloat16),
            jax.ShapeDtypeStruct((rows_dev, model_dim), jnp.bfloat16),
        ),
        in_specs=[vmem] * 7,
        out_specs=(vmem, vmem),
        scratch_shapes=[
            pltpu.VMEM((n_sp,) + kv.shape, jnp.bfloat16),
            pltpu.VMEM((n_sp,) + gates_docs.shape, jnp.float32),
            pltpu.VMEM((heads, tok_dev, 1), jnp.float32),
            pltpu.VMEM((heads, tok_dev, 1), jnp.float32),
            pltpu.VMEM((heads, tok_dev, head_size), jnp.float32),
            pltpu.VMEM((tok_dev, heads * head_size), jnp.bfloat16),
            pltpu.VMEM((n_tp, rows_dev, model_dim), jnp.bfloat16),
            pltpu.VMEM((n_tp, rows_dev, model_dim), jnp.bfloat16),
            dma((nz,)),
            dma((n_sp,)),
            dma((nz,)),
            dma((n_sp,)),
            dma((nz,)),
            dma((nz,)),
            dma((n_tp,)),
            dma((n_tp,)),
        ],
        compiler_params=pltpu.CompilerParams(
            collective_id=0, has_side_effects=True, vmem_limit_bytes=56 * 1024 * 1024
        ),
        name="attend",
    )(
        jnp.transpose(query_norm, (1, 0, 2)),
        kv,
        gates_docs,
        gates_docs.T,
        out_weight,
        residual,
        norm_gain[None, :],
    )

    experts = nz
    named = min(rows_dev, 6 * rows_dev // n_sp)
    capacity = named + (-named) % CHUNK
    expert_ids = jnp.arange(experts, dtype=jnp.int32)
    chosen = routes[:, :, None] == expert_ids[None, None, :]
    picked = jnp.sum(chosen.astype(jnp.float32), axis=1)
    weight_of = jnp.sum(jnp.where(chosen, route_weights[:, :, None], 0.0), axis=1)
    rank = jnp.cumsum(picked, axis=0) - 1.0
    slot_ids = jnp.arange(capacity).astype(jnp.float32)
    placing = picked.T[:, None, :] * (rank.T[:, None, :] == slot_ids[None, :, None]).astype(
        jnp.float32
    )
    outgoing = jnp.einsum(
        "ecr,rd->ecd", placing.astype(jnp.bfloat16), normed, preferred_element_type=jnp.float32
    ).astype(jnp.bfloat16)

    hidden_dev = w_gate.shape[2]
    block = (nz, capacity, model_dim)
    returned = pl.pallas_call(
        functools.partial(expert_kernel, nz, n_tp),
        out_shape=jax.ShapeDtypeStruct(block, jnp.bfloat16),
        in_specs=[vmem, hbm, hbm, hbm],
        out_specs=vmem,
        scratch_shapes=[
            pltpu.VMEM((model_dim, hidden_dev), jnp.bfloat16),
            pltpu.VMEM((model_dim, hidden_dev), jnp.bfloat16),
            pltpu.VMEM((hidden_dev, model_dim), jnp.bfloat16),
            pltpu.VMEM((nz, 2, n_tp) + block[1:], jnp.bfloat16),
            pltpu.VMEM((nz, 2, n_tp) + block[1:], jnp.bfloat16),
            pltpu.VMEM((nz, n_tp) + block[1:], jnp.bfloat16),
            pltpu.VMEM((nz, 2) + block[1:], jnp.bfloat16),
            pltpu.VMEM(block, jnp.bfloat16),
            pltpu.VMEM(block, jnp.bfloat16),
            dma((3,)),
            dma((nz,)),
            dma((nz,)),
            dma((3, nz)),
            dma((3, nz)),
            dma((nz,)),
            dma((nz,)),
            dma((n_tp, nz)),
            dma((n_tp, nz)),
            dma((nz,)),
            dma((nz,)),
            dma((nz,)),
            dma((nz,)),
            dma((2, nz)),
            dma((2, nz)),
            dma((nz,)),
            dma((nz,)),
        ],
        compiler_params=pltpu.CompilerParams(
            collective_id=1, has_side_effects=True, vmem_limit_bytes=60 * 1024 * 1024
        ),
        name="experts",
    )(outgoing, w_gate[0], w_up[0], w_down[0])

    combining = placing * weight_of.T[:, None, :]
    routed = jnp.einsum(
        "ecr,ecd->rd", combining, returned.astype(jnp.float32), precision=lax.Precision.HIGHEST
    )
    return (mixed.astype(jnp.float32) + routed).astype(jnp.bfloat16)


def solution(mesh):
    return jax.shard_map(
        functools.partial(local, mesh.shape["sp"] // 2, mesh.shape["tp"]),
        mesh=mesh,
        in_specs=(
            P(("grp", "sp"), "tp", None),
            P(("grp", "sp"), "tp", None),
            P(("grp", "sp"), "tp", None),
            P("tp", ("grp", "sp")),
            P(("grp", "sp")),
            P(),
            P(),
            P("tp", None),
            P(("grp", "sp", "tp"), None),
            P(),
            P(("grp", "sp", "tp"), None),
            P(("grp", "sp", "tp"), None),
            P("sp", None, "tp"),
            P("sp", None, "tp"),
            P("sp", "tp", None),
        ),
        out_specs=P(("grp", "sp", "tp"), None),
        check_vma=False,
    )
```

profile of v0, /device:TPU:0, one launch (start us, length us, event | category | flops | bytes accessed | tf_op | source)
XLA Modules:
  0.0 136.7 jit_solution(2993767806608110975)
XLA Ops:
  0.0 0.1 pad.2.clone
  0.1 0.7 convert_element_type.47
  0.8 0.9 fusion.8
  1.7 1.2 fusion.2
  2.9 0.7 select_reduce_fusion
  3.6 0.8 maximum_maximum_fusion.gd_ref
  4.4 0.0 copy-start.1
  4.4 0.1 copy.39
  4.5 0.1 reduce_window_sum.11
  4.6 0.1 copy.40
  4.7 1.0 fusion.10
  5.6 1.5 %pad_maximum_fusion.kv_ref = bf16[256,256]{1,0:T(8,128)(2,1)} fusion(bf16[256,128]{1,0:T(8,128)(2,1)} %bitcast.31, bf16[256,128]{1,0:T(8,128)(2,1)S(1)} %fusion.10), kind=kLoop, calls=%fused_computation.17 | loop fusion | flops 262144 | bytes 262144 | tf_op jit(solution)/shard_map/concatenate | solution.py:536
  7.1 0.8 copy.38
  7.9 1.9 %fusion.6.q_ref = bf16[4,256,128]{2,1,0:T(8,128)(2,1)} fusion(f32[128]{0:T(128)} %param.20, f32[256,4]{0,1:T(4,128)S(1)} %add_rsqrt_fusion, bf16[256,4,128]{2,1,0:T(4,128)(2,1)} %param.15), kind=kLoop, calls=%fused_computation.10 | loop fusion | flops 655360 | bytes 528896 | tf_op jit(solution)/shard_map/transpose | solution.py:580
  9.8 0.0 copy-done.1
  9.8 25.1 %attend.1 = (bf16[64,2048]{1,0:T(8,128)(2,1)}, bf16[64,2048]{1,0:T(8,128)(2,1)}) custom-call(bf16[4,256,128]{2,1,0:T(8,128)(2,1)} %fusion.6.q_ref, bf16[256,256]{1,0:T(8,128)(2,1)} %pad_maximum_fusion.kv_ref, f32[8,256]{1,0:T(8,128)} %copy-done.1, f32[256,8]{1,0:T(8,128)} %bitcast.30, bf16[512,2048]{1,0:T(8,128)(2,1)} %w_ref.1, bf16[64,2048]{1,0:T(8,128)(2,1)} %res_ref.1, ...), custom_call_target="tpu_custom_call" | custom-call | tf_op jit(solution)/shard_map/attend/pallas_call | solution.py:549
  34.9 2.2 %convolution_convert_fusion.out_ref = bf16[4,48,2048]{2,1,0:T(8,128)(2,1)} fusion(bf16[64,2048]{1,0:T(8,128)(2,1)} %get-tuple-element.8, f32[4,64]{1,0:T(4,128)S(1)} %bitcast.32, f32[4,64]{1,0:T(4,128)S(1)} %copy.40, f32[48]{0:T(128)S(1)} %iota_convert_fusion), kind=kOutput, calls=%fused_computation | convolution fusion | flops 50749440 | bytes 1050816 | tf_op jit(solution)/shard_map/ecr,rd->ecd/dot_general | solution.py:601
  37.1 0.0 copy-start
  37.1 97.0 %experts.1 = bf16[4,48,2048]{2,1,0:T(8,128)(2,1)} custom-call(bf16[4,48,2048]{2,1,0:T(8,128)(2,1)} %convolution_convert_fusion.out_ref, bf16[2048,512]{1,0:T(8,128)(2,1)} %bitcast.27, bf16[2048,512]{1,0:T(8,128)(2,1)} %bitcast.28, bf16[512,2048]{1,0:T(8,128)(2,1)} %bitcast.29), custom_call_target="tpu_custom_call" | custom-call | tf_op jit(solution)/shard_map/experts/pallas_call | solution.py:607
  134.2 0.0 copy-done
  134.2 2.5 %fusion.1 = bf16[64,2048]{1,0:T(8,128)(2,1)} fusion(bf16[4,48,2048]{2,1,0:T(8,128)(2,1)} %experts.1, bf16[64,2048]{1,0:T(8,128)(2,1)S(1)} %copy-done, f32[4,64]{1,0:T(4,128)S(1)} %bitcast.35, f32[4,64]{1,0:T(4,128)S(1)} %bitcast.33, f32[4,64]{1,0:T(4,128)S(1)} %copy.40, f32[48]{0:T(128)S(1)} %iota_convert_fusion), kind=kOutput, calls=%fused_computation.3 | convolution fusion | flops 302419968 | bytes 1313984 | tf_op jit(solution)/shard_map/ecr,ecd->rd/dot_general | solution.py:647
  (5 shorter events, 0.0 us)
Async XLA Ops:
  4.4 5.4 %copy-start.1 = (f32[8,256]{1,0:T(8,128)}, f32[8,256]{1,0:T(8,128)S(1)}, u32[]{:S(2)}) copy-start(f32[8,256]{1,0:T(8,128)S(1)} %maximum_maximum_fusion.gd_ref) | copy-start | bytes 24580
  37.1 97.0 %copy-start = (bf16[64,2048]{1,0:T(8,128)(2,1)S(1)}, bf16[64,2048]{1,0:T(8,128)(2,1)}, u32[]{:S(2)}) copy-start(bf16[64,2048]{1,0:T(8,128)(2,1)} %get-tuple-element.7) | copy-start | bytes 786436
where the time goes:
time: 137 us
  Pallas kernels  122 us (89%)
  other arithmetic  8.71 us (6%)
  matrix products  4.74 us (3%)
    pallas_call x1, Pallas kernels, local(): pl.pallas_call(functools.partial(expert_kernel, nz, n_tp), out_shape=jax....  97 us
    pallas_call x1, Pallas kernels, local(): pl.pallas_call(functools.partial(attend_kernel, nz, n_tp), out_shape=(jax...  25.1 us

commit v1 on v0

v1 whole, which is shorter than its diff:
```python
import functools

import jax
import jax.numpy as jnp
from jax import lax
from jax.experimental import pallas as pl
from jax.experimental.pallas import tpu as pltpu
from jax.sharding import PartitionSpec as P

EPSILON = 1e-06
CHUNK = 16
LIMBS = 3
MESH = pl.DeviceIdType.MESH
BF16 = jnp.bfloat16
F32 = jnp.float32


def rms_scale(inputs, gain):
    return inputs * lax.rsqrt(jnp.mean(inputs * inputs, axis=-1, keepdims=True) + EPSILON) * gain


def flip(index, bits, size):
    step = 1
    while step < size:
        bit = (bits // step) % 2
        index = index + bit * step * (1 - 2 * ((index // step) % 2))
        step *= 2
    return index


def remote(src, dst, send, recv, where):
    return pltpu.make_async_remote_copy(
        src, dst, send, recv, device_id=where, device_id_type=MESH
    )


def layer_kernel(
    nz,
    n_tp,
    q_ref,
    k_ref,
    v_ref,
    g_ref,
    d_ref,
    qg_ref,
    kg_ref,
    w_hbm,
    res_ref,
    gain_ref,
    rt_ref,
    rw_ref,
    wg_hbm,
    wu_hbm,
    wd_hbm,
    out_ref,
    w_ref,
    wg_ref,
    wu_ref,
    wd_ref,
    qf_ref,
    qt_ref,
    ext_ref,
    kx_ref,
    k_buf,
    v_buf,
    m_ref,
    l_ref,
    acc_ref,
    att_ref,
    sbuf,
    pho_buf,
    prs_buf,
    mixed_ref,
    normed_ref,
    out_buf,
    arrived,
    part,
    hbuf,
    rbuf,
    fin,
    ret,
    w_sem,
    wx_send,
    wx_recv,
    kc_send,
    vc_send,
    kx_send,
    vx_send,
    k_recv,
    v_recv,
    pho_send,
    pho_recv,
    prn_send,
    prn_recv,
    prf_send,
    prf_recv,
    a_send,
    a_recv,
    b_send,
    b_recv,
    f_send,
    f_recv,
    h_send,
    h_recv,
    r_send,
    r_recv,
    z_send,
    z_recv,
):
    s = lax.axis_index("sp")
    t = lax.axis_index("tp")
    z, c = s // 2, s % 2
    heads, rows, hd = acc_ref.shape[0], acc_ref.shape[2], acc_ref.shape[1]
    extra = ext_ref.shape[0]
    cap, width = out_buf.shape[1:]
    share = rows // n_tp
    half = share // 2
    partner = {"sp": 2 * z + 1 - c}
    near = 1 + c
    far = 2 - c
    near_at = flip(t, near, n_tp)
    far_at = flip(t, far, n_tp)
    to_near = {"tp": near_at}
    to_far = {"tp": far_at}

    barrier = pltpu.get_barrier_semaphore()
    for dz in range(1, nz):
        pl.semaphore_signal(
            barrier, inc=1, device_id={"sp": 2 * ((z + dz) % nz) + c}, device_id_type=MESH
        )
    for k in (1, 2):
        pl.semaphore_signal(
            barrier, inc=1, device_id={"tp": flip(t, k, n_tp)}, device_id_type=MESH
        )
    pl.semaphore_signal(barrier, inc=1, device_id=partner, device_id_type=MESH)
    loads = [
        pltpu.make_async_copy(src, dst, w_sem.at[i])
        for i, (src, dst) in enumerate(
            (
                (w_hbm, w_ref),
                (wg_hbm, wg_ref.at[0]),
                (wu_hbm, wu_ref.at[0]),
                (wd_hbm, wd_ref.at[0]),
            )
        )
    ]
    for load in loads:
        load.start()
    swaps = [
        remote(src, dst, wx_send.at[i], wx_recv.at[i], partner)
        for i, (src, dst) in enumerate(
            ((wg_hbm, wg_ref.at[1]), (wu_hbm, wu_ref.at[1]), (wd_hbm, wd_ref.at[1]))
        )
    ]

    k_buf[s] = rms_scale(k_ref[...].astype(F32), kg_ref[...]).astype(BF16)
    v_buf[s, 0:hd, :] = jnp.transpose(v_ref[...].astype(F32)).astype(BF16)
    gates = -g_ref[...]
    high = gates.astype(BF16).astype(F32)
    middle = (gates - high).astype(BF16).astype(F32)
    low = (gates - high - middle).astype(BF16).astype(F32)
    limbs = (high, middle, low)
    ext_ref[...] = jnp.zeros_like(ext_ref)
    for j, limb in enumerate(limbs):
        ext_ref[j * heads:(j + 1) * heads, :] = limb
    ones_at = LIMBS * heads
    doc_at = ones_at + LIMBS
    ext_ref[ones_at:ones_at + LIMBS, :] = jnp.ones((LIMBS, rows), F32)
    ext_ref[doc_at:doc_at + 1, :] = d_ref[...].astype(F32)
    v_buf[s, hd:hd + extra, :] = ext_ref[...].astype(BF16)

    pl.semaphore_wait(barrier, nz - 1 + 2 + 1)

    def chain(source, slot):
        there = {"sp": 2 * (z + 1) + c}
        return (
            remote(
                k_buf.at[source], k_buf.at[source], kc_send.at[slot], k_recv.at[source], there
            ),
            remote(
                v_buf.at[source], v_buf.at[source], vc_send.at[slot], v_recv.at[source], there
            ),
        )

    def across(source, slot):
        return (
            remote(
                k_buf.at[source], k_buf.at[source], kx_send.at[slot], k_recv.at[source], partner
            ),
            remote(
                v_buf.at[source], v_buf.at[source], vx_send.at[slot], v_recv.at[source], partner
            ),
        )

    @pl.when(z + 1 < nz)
    def _():
        for copy in chain(s, 0):
            copy.start()

    @pl.when(c == 0)
    def _():
        for copy in across(s, 0):
            copy.start()

    qf_ref[...] = q_ref[...].astype(F32)
    row = lax.broadcasted_iota(jnp.int32, (extra, rows), 0)
    for h in range(heads):
        picked = qf_ref[pl.ds(h, rows, stride=heads), :]
        query = (rms_scale(picked, qg_ref[...]) * hd ** (-0.5)).astype(BF16).astype(F32)
        qt_ref[h, 0:hd, :] = jnp.transpose(query).astype(BF16)
        mine = jnp.where((row < ones_at) & (row % heads == h), 1.0, 0.0)
        for j, limb in enumerate(limbs):
            mine = jnp.where(row == ones_at + j, -limb[h:h + 1, :], mine)
        qt_ref[h, hd:hd + extra, :] = mine.astype(BF16)
        qt_ref[h, hd + extra:, :] = jnp.zeros((hd - extra, rows), BF16)
    kx_ref[...] = jnp.zeros_like(kx_ref)
    here = d_ref[...].astype(F32)

    def update(source, own):
        kx_ref[0:extra, :] = v_buf[source, hd:hd + extra, :].astype(F32)
        columns = jnp.transpose(kx_ref[...])
        left = jnp.concatenate([k_buf[source], columns.astype(BF16)], axis=1)
        same = columns[:, doc_at:doc_at + 1] == here
        if own:
            key_at = lax.broadcasted_iota(jnp.int32, (rows, rows), 0)
            query_at = lax.broadcasted_iota(jnp.int32, (rows, rows), 1)
            same = same & (key_at <= query_at)
        for h in range(heads):
            scores = jnp.dot(left, qt_ref[h], preferred_element_type=F32)
            scores = jnp.where(same, scores, -jnp.inf)
            peak = jnp.max(scores, axis=0, keepdims=True)
            if own:
                new = peak
            else:
                old = m_ref[h]
                new = jnp.maximum(old, peak)
            expo = jnp.exp(scores - new)
            total = jnp.sum(expo, axis=0, keepdims=True)
            mix = jnp.dot(
                v_buf[source, 0:hd, :], expo.astype(BF16), preferred_element_type=F32
            )
            m_ref[h] = new
            if own:
                l_ref[h] = total
                acc_ref[h] = mix
            else:
                factor = jnp.exp(old - new)
                l_ref[h] = factor * l_ref[h] + total
                acc_ref[h] = factor * acc_ref[h] + mix

    update(s, True)

    def one_source(i, carry):
        dz = (i + 1) // 2
        direct = i % 2
        core = (1 - direct) * (1 - c) + direct * c
        source = 2 * (z - dz) + core
        for copy in across(source, dz):
            copy.wait_recv()

        @pl.when(direct == 1)
        def _():
            @pl.when(z + 1 < nz)
            def _():
                for copy in chain(source, dz):
                    copy.start()

            for copy in across(source, dz):
                copy.start()

        update(source, False)
        return carry

    lax.fori_loop(1 - c, 2 * z + 1, one_source, 0)

    for swap in swaps:
        swap.start()

    for h in range(heads):
        att_ref[:, h * hd:(h + 1) * hd] = jnp.transpose(acc_ref[h] / l_ref[h]).astype(BF16)

    def ho_copy(i):
        return remote(
            sbuf.at[3, pl.ds(i * half, half)], pho_buf.at[i], pho_send.at[i], pho_recv.at[i],
            to_near,
        )

    def rn_copy(i):
        return remote(
            sbuf.at[near, pl.ds(i * half, half)], prs_buf.at[0, pl.ds(i * half, half)],
            prn_send.at[i], prn_recv.at[i], to_near,
        )

    def rf_copy(i):
        return remote(
            sbuf.at[far, pl.ds(i * half, half)], prs_buf.at[1, pl.ds(i * half, half)],
            prf_send.at[i], prf_recv.at[i], to_far,
        )

    loads[0].wait()

    def project(k, column):
        start = pl.multiple_of(column * share, share)
        block = jnp.dot(
            att_ref[pl.ds(start, share), :], w_ref[...], preferred_element_type=F32
        )
        sbuf[k] = block.astype(BF16)

    def project_step(i, carry):
        k = (i == 0) * 3 + (i == 1) * near + (i == 2) * far
        project(k, flip(t, k, n_tp))

        @pl.when(i == 0)
        def _():
            for j in range(2):
                ho_copy(j).start()

        @pl.when(i == 1)
        def _():
            for j in range(2):
                rn_copy(j).start()

        return carry

    lax.fori_loop(0, n_tp, project_step, 0)

    for i in range(2):
        ho_copy(i).wait_recv()

        def pair(r, carry, i=i):
            at = pl.ds(pl.multiple_of(i * half + r * CHUNK, CHUNK), CHUNK)
            here_at = pl.ds(pl.multiple_of(r * CHUNK, CHUNK), CHUNK)
            total = sbuf[far, at, :].astype(F32) + pho_buf[i, here_at, :].astype(F32)
            sbuf[far, at, :] = total.astype(BF16)
            return carry

        lax.fori_loop(0, half // CHUNK, pair, 0)
        rf_copy(i).start()

    experts = nz
    padded = experts + (-experts) % 8
    n_slots = experts * cap
    first, second = rt_ref[0:1, :], rt_ref[1:2, :]
    names = lax.broadcasted_iota(jnp.int32, (padded, share), 0)
    chosen = [(names == first).astype(F32), (names == second).astype(F32)]
    up_to = lax.broadcasted_iota(jnp.int32, (share, share), 0) <= lax.broadcasted_iota(
        jnp.int32, (share, share), 1
    )
    rank = (
        jnp.dot(
            (chosen[0] + chosen[1]).astype(BF16),
            up_to.astype(F32).astype(BF16),
            preferred_element_type=F32,
        )
        - 1.0
    )
    start_of = names.astype(F32) * cap
    slots = [
        jnp.sum(choice * (rank + start_of), axis=0, keepdims=True) for choice in chosen
    ]
    slot_rows = lax.broadcasted_iota(jnp.int32, (n_slots, share), 0).astype(F32)
    placing = (
        (slot_rows == slots[0]).astype(F32) + (slot_rows == slots[1]).astype(F32)
    ).astype(BF16)
    diagonal = (
        lax.broadcasted_iota(jnp.int32, (share, share), 0)
        == lax.broadcasted_iota(jnp.int32, (share, share), 1)
    ).astype(F32)

    def column(values):
        return jnp.sum(diagonal * values, axis=1, keepdims=True)

    slot_columns = lax.broadcasted_iota(jnp.int32, (share, n_slots), 1).astype(F32)
    taking = [(slot_columns == column(slot)).astype(F32).astype(BF16) for slot in slots]
    weights = [column(rw_ref[k:k + 1, :]) for k in range(2)]

    for i in range(2):
        rn_copy(i).wait_recv()
        rf_copy(i).wait_recv()

        def finish(r, carry, i=i):
            at = pl.ds(pl.multiple_of(i * half + r * CHUNK, CHUNK), CHUNK)
            total = (
                sbuf[0, at, :].astype(F32)
                + prs_buf[0, at, :].astype(F32)
                + prs_buf[1, at, :].astype(F32)
            )
            mixed = (res_ref[at, :].astype(F32) + total).astype(BF16)
            mixed_ref[at, :] = mixed
            normed_ref[at, :] = rms_scale(mixed.astype(F32), gain_ref[...]).astype(BF16)
            return carry

        lax.fori_loop(0, half // CHUNK, finish, 0)

    out_buf[...] = (
        jnp.dot(placing, normed_ref[...], preferred_element_type=F32)
        .astype(BF16)
        .reshape(experts, cap, width)
    )

    def order(j):
        return j

    def along(e):
        return remote(
            out_buf.at[e], arrived.at[z, t], a_send.at[e], a_recv.at[z], {"sp": 2 * e + c}
        )

    def along_in(p):
        return remote(
            arrived.at[p, t], arrived.at[p, t], a_send.at[p], a_recv.at[p], partner
        )

    def spread(p, k):
        block = arrived.at[p, t]
        return remote(
            block, block, b_send.at[k, p], b_recv.at[k, p], to_far if k else to_near
        )

    def spread_in(p, k):
        block = arrived.at[p, far_at if k else near_at]
        return remote(block, block, b_send.at[k, p], b_recv.at[k, p], partner)

    def forward(p):
        block = arrived.at[p, far_at]
        return remote(block, block, f_send.at[p], f_recv.at[p], to_near)

    def forward_in(p):
        block = arrived.at[p, flip(t, 3, n_tp)]
        return remote(block, block, f_send.at[p], f_recv.at[p], partner)

    def hand_over(p):
        return remote(
            part.at[p, flip(t, 3, n_tp)], hbuf.at[p], h_send.at[p], h_recv.at[p], to_near
        )

    def reduce_near(p):
        return remote(
            part.at[p, near_at], rbuf.at[p, 0], r_send.at[0, p], r_recv.at[0, p], to_near
        )

    def reduce_far(p):
        return remote(
            part.at[p, far_at], rbuf.at[p, 1], r_send.at[1, p], r_recv.at[1, p], to_far
        )

    def home(p):
        return remote(
            fin.at[p], ret.at[z], z_send.at[p], z_recv.at[z], {"sp": 2 * p + c}
        )

    def home_in(e):
        return remote(fin.at[e], ret.at[e], z_send.at[e], z_recv.at[e], partner)

    def launch(p):
        @pl.when(p != z)
        def _():
            along_in(p).wait_recv()

        spread(p, 0).start()
        spread(p, 1).start()

    arrived[z, t] = out_buf[z]

    def send_out(dz, carry):
        along((z + dz) % nz).start()
        return carry

    lax.fori_loop(1, nz, send_out, 0)
    launch(order(0))
    for load in loads[1:]:
        load.wait()
    for swap in swaps:
        swap.wait_recv()

    def step(j, carry):
        @pl.when(j < nz)
        def _():
            p = order(j)
            spread_in(p, 1).wait_recv()
            forward(p).start()

        @pl.when(j + 1 < nz)
        def _():
            launch(order(j + 1))

        @pl.when((j >= 1) & (j <= nz))
        def _():
            p = order(j - 1)
            hand_over(p).wait_recv()

            def one(r, carry):
                at = pl.ds(pl.multiple_of(r * CHUNK, CHUNK), CHUNK)
                total = part[p, far_at, at, :].astype(F32) + hbuf[p, at, :].astype(F32)
                part[p, far_at, at, :] = total.astype(BF16)
                return carry

            lax.fori_loop(0, cap // CHUNK, one, 0)
            reduce_far(p).start()

        @pl.when(j < nz)
        def _():
            p = order(j)
            spread_in(p, 0).wait_recv()
            forward_in(p).wait_recv()
            flat = arrived[p].reshape(n_tp * cap, width)
            result = None
            for i in range(2):
                gate = jnp.dot(flat, wg_ref[i], preferred_element_type=F32)
                up = jnp.dot(flat, wu_ref[i], preferred_element_type=F32)
                hidden = (gate * (1.0 / (1.0 + jnp.exp(-gate))) * up).astype(BF16)
                down = jnp.dot(hidden, wd_ref[i], preferred_element_type=F32)
                result = down if result is None else result + down
            part[p] = result.astype(BF16).reshape(n_tp, cap, width)
            hand_over(p).start()
            reduce_near(p).start()

        @pl.when((j >= 2) & (j - 2 < nz))
        def _():
            p = order(j - 2)
            reduce_near(p).wait_recv()
            reduce_far(p).wait_recv()

            def one(r, carry):
                at = pl.ds(pl.multiple_of(r * CHUNK, CHUNK), CHUNK)
                total = (
                    part[p, t, at, :].astype(F32)
                    + rbuf[p, 0, at, :].astype(F32)
                    + rbuf[p, 1, at, :].astype(F32)
                )
                fin[p, at, :] = total.astype(BF16)
                return carry

            lax.fori_loop(0, cap // CHUNK, one, 0)

            @pl.when(p != z)
            def _():
                home(p).start()

            @pl.when(p == z)
            def _():
                ret[z] = fin[z]

        return carry

    lax.fori_loop(0, nz + 2, step, 0)

    def collect(dz, carry):
        home_in((z + dz) % nz).wait_recv()
        return carry

    lax.fori_loop(1, nz, collect, 0)

    both = jnp.concatenate(taking, axis=0)
    piece = width // 4
    for i in range(4):
        at = slice(i * piece, (i + 1) * piece)
        back = ret[:, :, at].reshape(n_slots, piece)
        rows_of = jnp.dot(both, back, preferred_element_type=F32)
        routed = weights[0] * rows_of[:share] + weights[1] * rows_of[share:]
        out_ref[:, at] = (mixed_ref[:, at].astype(F32) + routed).astype(BF16)

    def sent(dz, carry):
        p = (z + dz) % nz
        home(p).wait_send()
        along(p).wait_send()
        return carry

    lax.fori_loop(1, nz, sent, 0)

    def sent_plane(p, carry):
        for k in range(2):
            spread(p, k).wait_send()
        forward(p).wait_send()
        hand_over(p).wait_send()
        reduce_near(p).wait_send()
        reduce_far(p).wait_send()
        return carry

    lax.fori_loop(0, nz, sent_plane, 0)
    for i in range(2):
        ho_copy(i).wait_send()
        rn_copy(i).wait_send()
        rf_copy(i).wait_send()
    for swap in swaps:
        swap.wait_send()

    @pl.when(c == 0)
    def _():
        for copy in across(s, 0):
            copy.wait_send()

    @pl.when(z + 1 < nz)
    def _():
        for copy in chain(s, 0):
            copy.wait_send()

    def sent_source(dz, carry):
        source = 2 * (z - dz) + c
        for copy in across(source, dz):
            copy.wait_send()

        @pl.when(z + 1 < nz)
        def _():
            for copy in chain(source, dz):
                copy.wait_send()

        return carry

    lax.fori_loop(1, z + 1, sent_source, 0)


def local(
    nz,
    n_tp,
    queries,
    keys,
    values,
    log_gates,
    documents,
    query_gain,
    key_gain,
    out_weight,
    residual,
    norm_gain,
    routes,
    route_weights,
    w_gate,
    w_up,
    w_down,
):
    tok_dev, heads, hd = queries.shape
    rows_dev, width = residual.shape
    n_sp = 2 * nz
    named = min(rows_dev, 6 * rows_dev // n_sp)
    cap = named + (-named) % CHUNK
    hidden_dev = w_gate.shape[2]
    extra = LIMBS * heads + LIMBS + 1
    extra = extra + (-extra) % 16
    vmem = pl.BlockSpec(memory_space=pltpu.VMEM)
    hbm = pl.BlockSpec(memory_space=pl.ANY)
    dma = pltpu.SemaphoreType.DMA
    block = (cap, width)
    return pl.pallas_call(
        functools.partial(layer_kernel, nz, n_tp),
        out_shape=jax.ShapeDtypeStruct((rows_dev, width), BF16),
        in_specs=[vmem] * 7 + [hbm] + [vmem] * 4 + [hbm] * 3,
        out_specs=vmem,
        scratch_shapes=[
            pltpu.VMEM(out_weight.shape, BF16),
            pltpu.VMEM((2, width, hidden_dev), BF16),
            pltpu.VMEM((2, width, hidden_dev), BF16),
            pltpu.VMEM((2, hidden_dev, width), BF16),
            pltpu.VMEM((tok_dev * heads, hd), F32),
            pltpu.VMEM((heads, 2 * hd, tok_dev), BF16),
            pltpu.VMEM((extra, tok_dev), F32),
            pltpu.VMEM((hd, tok_dev), F32),
            pltpu.VMEM((n_sp, tok_dev, hd), BF16),
            pltpu.VMEM((n_sp, hd + extra, tok_dev), BF16),
            pltpu.VMEM((heads, 1, tok_dev), F32),
            pltpu.VMEM((heads, 1, tok_dev), F32),
            pltpu.VMEM((heads, hd, tok_dev), F32),
            pltpu.VMEM((tok_dev, heads * hd), BF16),
            pltpu.VMEM((n_tp, rows_dev, width), BF16),
            pltpu.VMEM((2, rows_dev // 2, width), BF16),
            pltpu.VMEM((2, rows_dev, width), BF16),
            pltpu.VMEM((rows_dev, width), BF16),
            pltpu.VMEM((rows_dev, width), BF16),
            pltpu.VMEM((nz,) + block, BF16),
            pltpu.VMEM((nz, n_tp) + block, BF16),
            pltpu.VMEM((nz, n_tp) + block, BF16),
            pltpu.VMEM((nz,) + block, BF16),
            pltpu.VMEM((nz, 2) + block, BF16),
            pltpu.VMEM((nz,) + block, BF16),
            pltpu.VMEM((nz,) + block, BF16),
            dma((4,)),
            dma((3,)),
            dma((3,)),
            dma((nz,)),
            dma((nz,)),
            dma((nz,)),
            dma((nz,)),
            dma((n_sp,)),
            dma((n_sp,)),
            dma((2,)),
            dma((2,)),
            dma((2,)),
            dma((2,)),
            dma((2,)),
            dma((2,)),
            dma((nz,)),
            dma((nz,)),
            dma((2, nz)),
            dma((2, nz)),
            dma((nz,)),
            dma((nz,)),
            dma((nz,)),
            dma((nz,)),
            dma((2, nz)),
            dma((2, nz)),
            dma((nz,)),
            dma((nz,)),
        ],
        compiler_params=pltpu.CompilerParams(
            collective_id=0, has_side_effects=True, vmem_limit_bytes=60 * 1024 * 1024
        ),
        name="layer",
    )(
        queries.reshape(tok_dev * heads, hd),
        keys.reshape(tok_dev, hd),
        values.reshape(tok_dev, hd),
        log_gates,
        documents[None, :],
        query_gain[None, :],
        key_gain[None, :],
        out_weight,
        residual,
        norm_gain[None, :],
        routes.T,
        route_weights.T,
        w_gate[0],
        w_up[0],
        w_down[0],
    )


def solution(mesh):
    return jax.shard_map(
        functools.partial(local, mesh.shape["sp"] // 2, mesh.shape["tp"]),
        mesh=mesh,
        in_specs=(
            P(("grp", "sp"), "tp", None),
            P(("grp", "sp"), "tp", None),
            P(("grp", "sp"), "tp", None),
            P("tp", ("grp", "sp")),
            P(("grp", "sp")),
            P(),
            P(),
            P("tp", None),
            P(("grp", "sp", "tp"), None),
            P(),
            P(("grp", "sp", "tp"), None),
            P(("grp", "sp", "tp"), None),
            P("sp", None, "tp"),
            P("sp", None, "tp"),
            P("sp", "tp", None),
        ),
        out_specs=P(("grp", "sp", "tp"), None),
        check_vma=False,
    )
```

time: 137 us -> 105 us (0.77)
  the two profiles are of different devices: /device:TPU:0 before, /device:TPU:24 now
where the time goes in v1:
time: 105 us
  Pallas kernels  103 us (98%)
  local copies, waits for them, and re-layouts  1.67 us (2%)
    pallas_call x1, Pallas kernels, local(): pl.pallas_call(functools.partial(layer_kernel, nz, n_tp), out_shape=jax.S...  103 us

profile of v1, /device:TPU:24, one launch (start us, length us, event | category | flops | bytes accessed | tf_op | source)
XLA Modules:
  0.0 104.9 jit_solution(7369564555106361027)
XLA Ops:
  0.0 103.2 %layer.1 = bf16[64,2048]{1,0:T(8,128)(2,1)} custom-call(bf16[1024,128]{1,0:T(8,128)(2,1)} %bitcast.15, bf16[256,128]{1,0:T(8,128)(2,1)} %bitcast.16, bf16[256,128]{1,0:T(8,128)(2,1)} %bitcast.17, f32[4,256]{1,0:T(4,128)} %g_ref.1, s32[1,256]{1,0:T(1,128)} %bitcast.19, f32[1,128]{1,0:T(1,128)} %bitcast.22, f32[1,128]{1,0:T(1,128)} %bitcast.23, ...), custom_call_target="tpu_custom_call" | custom-call | tf_op jit(solution)/shard_map/layer/pallas_call | solution.py:644
  103.3 1.7 %copy.17 = bf16[64,2048]{1,0:T(8,128)(2,1)} copy(bf16[64,2048]{1,0:T(8,128)(2,1)} %layer.1) | data formatting | bytes 524288

commit v2 on v1

--- a/solution.py
+++ b/solution.py
@@ -255,18 +255,18 @@
         direct = i % 2
         core = (1 - direct) * (1 - c) + direct * c
         source = 2 * (z - dz) + core
-        for copy in across(source, dz):
-            copy.wait_recv()
-
-        @pl.when(direct == 1)
-        def _():
-            @pl.when(z + 1 < nz)
-            def _():
-                for copy in chain(source, dz):
-                    copy.start()
-
-            for copy in across(source, dz):
-                copy.start()
+        onward = chain(source, dz)
+        aside = across(source, dz)
+        for k in range(2):
+            aside[k].wait_recv()
+
+            @pl.when(direct == 1)
+            def _(k=k):
+                @pl.when(z + 1 < nz)
+                def _():
+                    onward[k].start()
+
+                aside[k].start()
 
         update(source, False)
         return carry
@@ -398,8 +398,14 @@
         .reshape(experts, cap, width)
     )
 
+    upper = 2 * z // nz
+    ahead = (z + nz - 1) // nz
+
     def order(j):
-        return j
+        return (j <= z) * (z - j) + (j > z) * j
+
+    def turn(j):
+        return order((j + ahead) % nz)
 
     def along(e):
         return remote(
@@ -463,44 +469,58 @@
     arrived[z, t] = out_buf[z]
 
     def send_out(dz, carry):
-        along((z + dz) % nz).start()
+        @pl.when(z - dz >= 0)
+        def _():
+            along(z - dz).start()
+
+        @pl.when(z + dz < nz)
+        def _():
+            along(z + dz).start()
+
         return carry
 
-    lax.fori_loop(1, nz, send_out, 0)
+    def pass_on(p):
+        spread_in(p, 1).wait_recv()
+        forward(p).start()
+
+    send_out(1, 0)
     launch(order(0))
+
+    @pl.when(ahead == 0)
+    def _():
+        pass_on(order(0))
+
+    launch(order(1))
+    lax.fori_loop(2, min(nz, 3), send_out, 0)
+
+    @pl.when(ahead == 1)
+    def _():
+        pass_on(order(0))
+
+    lax.fori_loop(3, nz, send_out, 0)
+
+    @pl.when(ahead == 1)
+    def _():
+        pass_on(order(1))
+        launch(order(2))
+
     for load in loads[1:]:
         load.wait()
     for swap in swaps:
         swap.wait_recv()
 
     def step(j, carry):
+        @pl.when((j + 3 < nz) & (upper == 1))
+        def _():
+            launch(order(j + 3))
+
+        @pl.when((j + 2 < nz) & (ahead == 1))
+        def _():
+            pass_on(order(j + 2))
+
         @pl.when(j < nz)
         def _():
-            p = order(j)
-            spread_in(p, 1).wait_recv()
-            forward(p).start()
-
-        @pl.when(j + 1 < nz)
-        def _():
-            launch(order(j + 1))
-
-        @pl.when((j >= 1) & (j <= nz))
-        def _():
-            p = order(j - 1)
-            hand_over(p).wait_recv()
-
-            def one(r, carry):
-                at = pl.ds(pl.multiple_of(r * CHUNK, CHUNK), CHUNK)
-                total = part[p, far_at, at, :].astype(F32) + hbuf[p, at, :].astype(F32)
-                part[p, far_at, at, :] = total.astype(BF16)
-                return carry
-
-            lax.fori_loop(0, cap // CHUNK, one, 0)
-            reduce_far(p).start()
-
-        @pl.when(j < nz)
-        def _():
-            p = order(j)
+            p = turn(j)
             spread_in(p, 0).wait_recv()
             forward_in(p).wait_recv()
             flat = arrived[p].reshape(n_tp * cap, width)
@@ -513,11 +533,44 @@
                 result = down if result is None else result + down
             part[p] = result.astype(BF16).reshape(n_tp, cap, width)
             hand_over(p).start()
-            reduce_near(p).start()
+
+            @pl.when((j < nz - 2) & (ahead == 1))
+            def _():
+                reduce_near(p).start()
+
+        @pl.when((j + 1 < nz) & (ahead == 0))
+        def _():
+            pass_on(order(j + 1))
+
+        @pl.when((j + 2 < nz) & (ahead == 0))
+        def _():
+            launch(order(j + 2))
+
+        @pl.when((j >= 1) & (j <= nz))
+        def _():
+            p = turn(j - 1)
+            hand_over(p).wait_recv()
+
+            def one(r, carry):
+                at = pl.ds(pl.multiple_of(r * CHUNK, CHUNK), CHUNK)
+                total = part[p, far_at, at, :].astype(F32) + hbuf[p, at, :].astype(F32)
+                part[p, far_at, at, :] = total.astype(BF16)
+                return carry
+
+            lax.fori_loop(0, cap // CHUNK, one, 0)
+            reduce_far(p).start()
+
+            @pl.when((j > nz - 2) | (ahead == 0))
+            def _():
+                reduce_near(p).start()
+
+        @pl.when((j + 3 < nz) & (upper == 0) & (ahead == 1))
+        def _():
+            launch(order(j + 3))
 
         @pl.when((j >= 2) & (j - 2 < nz))
         def _():
-            p = order(j - 2)
+            p = turn(j - 2)
             reduce_near(p).wait_recv()
             reduce_far(p).wait_recv()
 

time: 105 us -> 93.5 us (0.89); the launches traced: 105 us -> 91.8 us
  Pallas kernels: 103 us -> 90.1 us
    pallas_call x1, Pallas kernels: 103 us -> 90.1 us  [local(): pl.pallas_call(functools.partial(layer_kernel, nz, n_tp), out_shape=jax.S...]
where the time goes in v2:
time: 93.5 us; the launch traced here: 91.8 us
  Pallas kernels  90.1 us (96%)
  local copies, waits for them, and re-layouts  1.67 us (2%)
    pallas_call x1, Pallas kernels, local(): pl.pallas_call(functools.partial(layer_kernel, nz, n_tp), out_shape=jax.S...  90.1 us

profile of v2, /device:TPU:24, one launch (start us, length us, event | category | flops | bytes accessed | tf_op | source)
XLA Modules:
  0.0 91.8 jit_solution(2621411555810785218)
XLA Ops:
  0.0 90.1 %layer.1 = bf16[64,2048]{1,0:T(8,128)(2,1)} custom-call(bf16[1024,128]{1,0:T(8,128)(2,1)} %bitcast.15, bf16[256,128]{1,0:T(8,128)(2,1)} %bitcast.16, bf16[256,128]{1,0:T(8,128)(2,1)} %bitcast.17, f32[4,256]{1,0:T(4,128)} %g_ref.1, s32[1,256]{1,0:T(1,128)} %bitcast.19, f32[1,128]{1,0:T(1,128)} %bitcast.22, f32[1,128]{1,0:T(1,128)} %bitcast.23, ...), custom_call_target="tpu_custom_call" | custom-call | tf_op jit(solution)/shard_map/layer/pallas_call | solution.py:697
  90.1 1.7 %copy.17 = bf16[64,2048]{1,0:T(8,128)(2,1)} copy(bf16[64,2048]{1,0:T(8,128)(2,1)} %layer.1) | data formatting | bytes 524288

commit v3 on v2

--- a/solution.py
+++ b/solution.py
@@ -32,6 +32,47 @@
     return pltpu.make_async_remote_copy(
         src, dst, send, recv, device_id=where, device_id_type=MESH
     )
+
+
+KINDS = "LFCDRESN"
+WORD = 10
+PLANS = (
+    ("SLFLSCFSLCFLDRFCDRCEDREDREE", "0123", "0123", "123", "123"),
+    ("SLFLSCFSLCFLDRFCDRCEDREDREE", "0123", "0123", "123", "123"),
+    ("SSLLFSFLFCRLFCRDCDECDREDREE", "1023", "0231", "023", "023"),
+    ("SSLLFSFLFCRLFCRDCDECDREDREE", "1023", "0231", "023", "023"),
+    ("SSSLLFFLLFCRFCRDCDECDREDREE", "2103", "1032", "310", "103"),
+    ("SSSLLFFLLFCRFCRDCDECDREDREE", "2103", "1032", "310", "103"),
+    ("SLLFSFSLLFCRFCRDCDECDREDREE", "3201", "2013", "201", "012"),
+    ("SLLFSFSLLFCRFCRDCDECDREDREE", "3201", "2013", "201", "012"),
+)
+
+
+def plan(nz, s):
+    if 2 * nz == len(PLANS):
+        text, *lists = PLANS[s]
+        return [text] + [[int(plane) for plane in planes] for planes in lists]
+    z = s // 2
+    text = "S" * (nz - 1) + "L" + "FL" * (nz - 1) + "F" + "CRD" * nz + "E" * nz
+    planes = [(z + dz) % nz for dz in range(nz)]
+    return [text, planes, planes[1:] + planes[:1], planes[1:], planes[1:]]
+
+
+def packed(text):
+    words = []
+    for at in range(0, len(text), WORD):
+        word = 0
+        for kind in reversed(text[at:at + WORD]):
+            word = word * len(KINDS) + KINDS.index(kind)
+        words.append(word)
+    return words
+
+
+def chosen_by(index, values):
+    total = 0
+    for i, value in enumerate(values):
+        total = total + (index == i) * value
+    return total
 
 
 def layer_kernel(
@@ -79,6 +120,7 @@
     rbuf,
     fin,
     ret,
+    rout_ref,
     w_sem,
     wx_send,
     wx_recv,
@@ -207,12 +249,13 @@
     for h in range(heads):
         picked = qf_ref[pl.ds(h, rows, stride=heads), :]
         query = (rms_scale(picked, qg_ref[...]) * hd ** (-0.5)).astype(BF16).astype(F32)
-        qt_ref[h, 0:hd, :] = jnp.transpose(query).astype(BF16)
+        lanes = slice(h * rows, (h + 1) * rows)
+        qt_ref[0:hd, lanes] = jnp.transpose(query).astype(BF16)
         mine = jnp.where((row < ones_at) & (row % heads == h), 1.0, 0.0)
         for j, limb in enumerate(limbs):
             mine = jnp.where(row == ones_at + j, -limb[h:h + 1, :], mine)
-        qt_ref[h, hd:hd + extra, :] = mine.astype(BF16)
-        qt_ref[h, hd + extra:, :] = jnp.zeros((hd - extra, rows), BF16)
+        qt_ref[hd:hd + extra, lanes] = mine.astype(BF16)
+        qt_ref[hd + extra:, lanes] = jnp.zeros((hd - extra, rows), BF16)
     kx_ref[...] = jnp.zeros_like(kx_ref)
     here = d_ref[...].astype(F32)
 
@@ -225,28 +268,31 @@
             key_at = lax.broadcasted_iota(jnp.int32, (rows, rows), 0)
             query_at = lax.broadcasted_iota(jnp.int32, (rows, rows), 1)
             same = same & (key_at <= query_at)
+        products = jnp.dot(left, qt_ref[...], preferred_element_type=F32)
+        expos = []
+        factors = []
         for h in range(heads):
-            scores = jnp.dot(left, qt_ref[h], preferred_element_type=F32)
-            scores = jnp.where(same, scores, -jnp.inf)
+            scores = jnp.where(same, products[:, h * rows:(h + 1) * rows], -jnp.inf)
             peak = jnp.max(scores, axis=0, keepdims=True)
             if own:
                 new = peak
             else:
                 old = m_ref[h]
                 new = jnp.maximum(old, peak)
+                factors.append(jnp.exp(old - new))
             expo = jnp.exp(scores - new)
             total = jnp.sum(expo, axis=0, keepdims=True)
-            mix = jnp.dot(
-                v_buf[source, 0:hd, :], expo.astype(BF16), preferred_element_type=F32
-            )
             m_ref[h] = new
-            if own:
-                l_ref[h] = total
-                acc_ref[h] = mix
-            else:
-                factor = jnp.exp(old - new)
-                l_ref[h] = factor * l_ref[h] + total
-                acc_ref[h] = factor * acc_ref[h] + mix
+            l_ref[h] = total if own else factors[h] * l_ref[h] + total
+            expos.append(expo.astype(BF16))
+        mixes = jnp.dot(
+            v_buf[source, 0:hd, :],
+            jnp.concatenate(expos, axis=1),
+            preferred_element_type=F32,
+        )
+        for h in range(heads):
+            mix = mixes[:, h * rows:(h + 1) * rows]
+            acc_ref[h] = mix if own else factors[h] * acc_ref[h] + mix
 
     update(s, True)
 
@@ -277,7 +323,7 @@
         swap.start()
 
     for h in range(heads):
-        att_ref[:, h * hd:(h + 1) * hd] = jnp.transpose(acc_ref[h] / l_ref[h]).astype(BF16)
+        att_ref[:, h * hd:(h + 1) * hd] = jnp.transpose(acc_ref[h] * (1.0 / l_ref[h])).astype(BF16)
 
     def ho_copy(i):
         return remote(
@@ -370,8 +416,7 @@
     def column(values):
         return jnp.sum(diagonal * values, axis=1, keepdims=True)
 
-    slot_columns = lax.broadcasted_iota(jnp.int32, (share, n_slots), 1).astype(F32)
-    taking = [(slot_columns == column(slot)).astype(F32).astype(BF16) for slot in slots]
+    slot_of = jnp.concatenate([column(slot) for slot in slots], axis=0)
     weights = [column(rw_ref[k:k + 1, :]) for k in range(2)]
 
     for i in range(2):
@@ -398,14 +443,24 @@
         .reshape(experts, cap, width)
     )
 
-    upper = 2 * z // nz
-    ahead = (z + nz - 1) // nz
+    plans = [plan(nz, i) for i in range(2 * nz)]
+    longest = max(len(text) for text, *_ in plans)
+    codes = [packed(text) for text, *_ in plans]
+    codes = [
+        chosen_by(s, [words[i] if i < len(words) else 0 for words in codes])
+        for i in range(-(-longest // WORD))
+    ]
+    length = chosen_by(s, [len(text) for text, *_ in plans])
+    orders, turns, targets, backs = (
+        [chosen_by(s, planes) for planes in zip(*lists)]
+        for lists in list(zip(*plans))[1:]
+    )
 
     def order(j):
-        return (j <= z) * (z - j) + (j > z) * j
+        return chosen_by(j, orders)
 
     def turn(j):
-        return order((j + ahead) % nz)
+        return chosen_by(j, turns)
 
     def along(e):
         return remote(
@@ -468,150 +523,121 @@
 
     arrived[z, t] = out_buf[z]
 
-    def send_out(dz, carry):
-        @pl.when(z - dz >= 0)
-        def _():
-            along(z - dz).start()
-
-        @pl.when(z + dz < nz)
-        def _():
-            along(z + dz).start()
-
-        return carry
-
     def pass_on(p):
         spread_in(p, 1).wait_recv()
         forward(p).start()
 
-    send_out(1, 0)
-    launch(order(0))
-
-    @pl.when(ahead == 0)
-    def _():
-        pass_on(order(0))
-
-    launch(order(1))
-    lax.fori_loop(2, min(nz, 3), send_out, 0)
-
-    @pl.when(ahead == 1)
-    def _():
-        pass_on(order(0))
-
-    lax.fori_loop(3, nz, send_out, 0)
-
-    @pl.when(ahead == 1)
-    def _():
-        pass_on(order(1))
-        launch(order(2))
-
     for load in loads[1:]:
         load.wait()
-    for swap in swaps:
-        swap.wait_recv()
-
-    def step(j, carry):
-        @pl.when((j + 3 < nz) & (upper == 1))
+
+    def compute(p, index):
+        @pl.when(index == 0)
         def _():
-            launch(order(j + 3))
-
-        @pl.when((j + 2 < nz) & (ahead == 1))
+            for swap in swaps:
+                swap.wait_recv()
+
+        spread_in(p, 0).wait_recv()
+        forward_in(p).wait_recv()
+        flat = arrived[p].reshape(n_tp * cap, width)
+        result = None
+        for i in range(2):
+            gate = jnp.dot(flat, wg_ref[i], preferred_element_type=F32)
+            up = jnp.dot(flat, wu_ref[i], preferred_element_type=F32)
+            hidden = (gate * (1.0 / (1.0 + jnp.exp(-gate))) * up).astype(BF16)
+            down = jnp.dot(hidden, wd_ref[i], preferred_element_type=F32)
+            result = down if result is None else result + down
+        part[p] = result.astype(BF16).reshape(n_tp, cap, width)
+        hand_over(p).start()
+
+    def add_far(p):
+        hand_over(p).wait_recv()
+
+        def one(r, carry):
+            at = pl.ds(pl.multiple_of(r * CHUNK, CHUNK), CHUNK)
+            total = part[p, far_at, at, :].astype(F32) + hbuf[p, at, :].astype(F32)
+            part[p, far_at, at, :] = total.astype(BF16)
+            return carry
+
+        lax.fori_loop(0, cap // CHUNK, one, 0)
+        reduce_far(p).start()
+
+    def end(p):
+        reduce_near(p).wait_recv()
+        reduce_far(p).wait_recv()
+
+        def one(r, carry):
+            at = pl.ds(pl.multiple_of(r * CHUNK, CHUNK), CHUNK)
+            total = (
+                part[p, t, at, :].astype(F32)
+                + rbuf[p, 0, at, :].astype(F32)
+                + rbuf[p, 1, at, :].astype(F32)
+            )
+            fin[p, at, :] = total.astype(BF16)
+            return carry
+
+        lax.fori_loop(0, cap // CHUNK, one, 0)
+
+        @pl.when(p != z)
         def _():
-            pass_on(order(j + 2))
-
-        @pl.when(j < nz)
+            home(p).start()
+
+        @pl.when(p == z)
         def _():
-            p = turn(j)
-            spread_in(p, 0).wait_recv()
-            forward_in(p).wait_recv()
-            flat = arrived[p].reshape(n_tp * cap, width)
-            result = None
-            for i in range(2):
-                gate = jnp.dot(flat, wg_ref[i], preferred_element_type=F32)
-                up = jnp.dot(flat, wu_ref[i], preferred_element_type=F32)
-                hidden = (gate * (1.0 / (1.0 + jnp.exp(-gate))) * up).astype(BF16)
-                down = jnp.dot(hidden, wd_ref[i], preferred_element_type=F32)
-                result = down if result is None else result + down
-            part[p] = result.astype(BF16).reshape(n_tp, cap, width)
-            hand_over(p).start()
-
-            @pl.when((j < nz - 2) & (ahead == 1))
-            def _():
-                reduce_near(p).start()
-
-        @pl.when((j + 1 < nz) & (ahead == 0))
-        def _():
-            pass_on(order(j + 1))
-
-        @pl.when((j + 2 < nz) & (ahead == 0))
-        def _():
-            launch(order(j + 2))
-
-        @pl.when((j >= 1) & (j <= nz))
-        def _():
-            p = turn(j - 1)
-            hand_over(p).wait_recv()
-
-            def one(r, carry):
-                at = pl.ds(pl.multiple_of(r * CHUNK, CHUNK), CHUNK)
-                total = part[p, far_at, at, :].astype(F32) + hbuf[p, at, :].astype(F32)
-                part[p, far_at, at, :] = total.astype(BF16)
-                return carry
-
-            lax.fori_loop(0, cap // CHUNK, one, 0)
-            reduce_far(p).start()
-
-            @pl.when((j > nz - 2) | (ahead == 0))
-            def _():
-                reduce_near(p).start()
-
-        @pl.when((j + 3 < nz) & (upper == 0) & (ahead == 1))
-        def _():
-            launch(order(j + 3))
-
-        @pl.when((j >= 2) & (j - 2 < nz))
-        def _():
-            p = turn(j - 2)
-            reduce_near(p).wait_recv()
-            reduce_far(p).wait_recv()
-
-            def one(r, carry):
-                at = pl.ds(pl.multiple_of(r * CHUNK, CHUNK), CHUNK)
-                total = (
-                    part[p, t, at, :].astype(F32)
-                    + rbuf[p, 0, at, :].astype(F32)
-                    + rbuf[p, 1, at, :].astype(F32)
-                )
-                fin[p, at, :] = total.astype(BF16)
-                return carry
-
-            lax.fori_loop(0, cap // CHUNK, one, 0)
-
-            @pl.when(p != z)
-            def _():
-                home(p).start()
-
-            @pl.when(p == z)
-            def _():
-                ret[z] = fin[z]
-
+            ret[z] = fin[z]
+
+    doing = {
+        "L": lambda j: launch(order(j)),
+        "F": lambda j: pass_on(order(j)),
+        "C": lambda j: compute(turn(j), j),
+        "D": lambda j: add_far(turn(j)),
+        "R": lambda j: reduce_near(turn(j)).start(),
+        "E": lambda j: end(turn(j)),
+        "S": lambda j: along(chosen_by(j, targets)).start(),
+    }
+
+    def tick(i, carry):
+        code, counts = carry
+        fresh = (i % WORD) == 0
+        code = jnp.where(fresh, chosen_by(i // WORD, codes), code // len(KINDS))
+        kind = code % len(KINDS)
+        for k, name in enumerate(KINDS[:len(doing)]):
+            @pl.when(kind == k)
+            def _(k=k, name=name):
+                doing[name](counts[k])
+
+        counts = tuple(count + (kind == k) for k, count in enumerate(counts))
+        return code, counts
+
+    zero = jnp.int32(0)
+    lax.fori_loop(0, length, tick, (zero, (zero,) * len(KINDS)))
+
+    numbers = lax.broadcasted_iota(jnp.int32, (2 * share, cap), 1).astype(F32)
+    piece = width // 4
+
+    def gather(e, finish):
+        taking = (numbers + (e * cap).astype(F32) == slot_of).astype(F32).astype(BF16)
+        for i in range(4):
+            at = slice(i * piece, (i + 1) * piece)
+            found = jnp.dot(taking, ret[e, :, at], preferred_element_type=F32)
+            routed = rout_ref[:, at] + weights[0] * found[:share] + weights[1] * found[share:]
+            if finish:
+                out_ref[:, at] = (mixed_ref[:, at].astype(F32) + routed).astype(BF16)
+            else:
+                rout_ref[:, at] = routed
+
+    rout_ref[...] = jnp.zeros_like(rout_ref)
+    gather(z, False)
+
+    def collect(i, carry):
+        e = chosen_by(i, backs)
+        home_in(e).wait_recv()
+        gather(e, False)
         return carry
 
-    lax.fori_loop(0, nz + 2, step, 0)
-
-    def collect(dz, carry):
-        home_in((z + dz) % nz).wait_recv()
-        return carry
-
-    lax.fori_loop(1, nz, collect, 0)
-
-    both = jnp.concatenate(taking, axis=0)
-    piece = width // 4
-    for i in range(4):
-        at = slice(i * piece, (i + 1) * piece)
-        back = ret[:, :, at].reshape(n_slots, piece)
-        rows_of = jnp.dot(both, back, preferred_element_type=F32)
-        routed = weights[0] * rows_of[:share] + weights[1] * rows_of[share:]
-        out_ref[:, at] = (mixed_ref[:, at].astype(F32) + routed).astype(BF16)
+    lax.fori_loop(0, nz - 2, collect, 0)
+    final = backs[nz - 2]
+    home_in(final).wait_recv()
+    gather(final, True)
 
     def sent(dz, carry):
         p = (z + dz) % nz
@@ -705,7 +731,7 @@
             pltpu.VMEM((2, width, hidden_dev), BF16),
             pltpu.VMEM((2, hidden_dev, width), BF16),
             pltpu.VMEM((tok_dev * heads, hd), F32),
-            pltpu.VMEM((heads, 2 * hd, tok_dev), BF16),
+            pltpu.VMEM((2 * hd, heads * tok_dev), BF16),
             pltpu.VMEM((extra, tok_dev), F32),
             pltpu.VMEM((hd, tok_dev), F32),
             pltpu.VMEM((n_sp, tok_dev, hd), BF16),
@@ -726,6 +752,7 @@
             pltpu.VMEM((nz, 2) + block, BF16),
             pltpu.VMEM((nz,) + block, BF16),
             pltpu.VMEM((nz,) + block, BF16),
+            pltpu.VMEM((rows_dev, width), F32),
             dma((4,)),
             dma((3,)),
             dma((3,)),

time: 93.5 us -> 91 us (0.973); the launches traced: 91.8 us -> 90.9 us
  no operation moved by 1% of the time
where the time goes in v3:
time: 91 us; the launch traced here: 90.9 us
  Pallas kernels  89.2 us (98%)
  local copies, waits for them, and re-layouts  1.67 us (2%)
    pallas_call x1, Pallas kernels, local(): pl.pallas_call(functools.partial(layer_kernel, nz, n_tp), out_shape=jax.S...  89.2 us

profile of v3, /device:TPU:24, one launch (start us, length us, event | category | flops | bytes accessed | tf_op | source)
XLA Modules:
  0.0 90.9 jit_solution(7592324046391693999)
XLA Ops:
  0.0 89.2 %layer.1 = bf16[64,2048]{1,0:T(8,128)(2,1)} custom-call(bf16[1024,128]{1,0:T(8,128)(2,1)} %bitcast.15, bf16[256,128]{1,0:T(8,128)(2,1)} %bitcast.16, bf16[256,128]{1,0:T(8,128)(2,1)} %bitcast.17, f32[4,256]{1,0:T(4,128)} %g_ref.1, s32[1,256]{1,0:T(1,128)} %bitcast.19, f32[1,128]{1,0:T(1,128)} %bitcast.22, f32[1,128]{1,0:T(1,128)} %bitcast.23, ...), custom_call_target="tpu_custom_call" | custom-call | tf_op jit(solution)/shard_map/layer/pallas_call | solution.py:723
  89.2 1.7 %copy.17 = bf16[64,2048]{1,0:T(8,128)(2,1)} copy(bf16[64,2048]{1,0:T(8,128)(2,1)} %layer.1) | data formatting | bytes 524288

commit v4 on v3

--- a/solution.py
+++ b/solution.py
@@ -39,10 +39,10 @@
 PLANS = (
     ("SLFLSCFSLCFLDRFCDRCEDREDREE", "0123", "0123", "123", "123"),
     ("SLFLSCFSLCFLDRFCDRCEDREDREE", "0123", "0123", "123", "123"),
-    ("SSLLFSFLFCRLFCRDCDECDREDREE", "1023", "0231", "023", "023"),
-    ("SSLLFSFLFCRLFCRDCDECDREDREE", "1023", "0231", "023", "023"),
-    ("SSSLLFFLLFCRFCRDCDECDREDREE", "2103", "1032", "310", "103"),
-    ("SSSLLFFLLFCRFCRDCDECDREDREE", "2103", "1032", "310", "103"),
+    ("SSLLFSFLFCRLFCRDCDEDRECEDRE", "1023", "0231", "023", "023"),
+    ("SSLLFSFLFCRLFCRDCDEDRECEDRE", "1023", "0231", "023", "023"),
+    ("SSSLLFFLLFCRFCRDCDEDRECEDRE", "2103", "1032", "310", "103"),
+    ("SSSLLFFLLFCRFCRDCDEDRECEDRE", "2103", "1032", "310", "103"),
     ("SLLFSFSLLFCRFCRDCDECDREDREE", "3201", "2013", "201", "012"),
     ("SLLFSFSLLFCRFCRDCDECDREDREE", "3201", "2013", "201", "012"),
 )
@@ -75,9 +75,23 @@
     return total
 
 
+def entry(nz, n_tp, *refs):
+    small = refs[:7] + refs[8:12]
+    held = refs[16:16 + len(small)]
+    fills = [
+        pltpu.make_async_copy(src, dst, refs[-1].at[i])
+        for i, (src, dst) in enumerate(zip(small, held))
+    ]
+    layer_kernel(
+        nz, n_tp, fills, *held[:7], refs[7], *held[7:], *refs[12:16],
+        *refs[16 + len(small):-1],
+    )
+
+
 def layer_kernel(
     nz,
     n_tp,
+    fills,
     q_ref,
     k_ref,
     v_ref,
@@ -186,8 +200,12 @@
             )
         )
     ]
-    for load in loads:
-        load.start()
+    first = (1, 2, 3, 4, 6)
+    for i in first:
+        fills[i].start()
+    for i, fill in enumerate(fills):
+        if i not in first:
+            fill.start()
     swaps = [
         remote(src, dst, wx_send.at[i], wx_recv.at[i], partner)
         for i, (src, dst) in enumerate(
@@ -195,6 +213,8 @@
         )
     ]
 
+    for i in first:
+        fills[i].wait()
     k_buf[s] = rms_scale(k_ref[...].astype(F32), kg_ref[...]).astype(BF16)
     v_buf[s, 0:hd, :] = jnp.transpose(v_ref[...].astype(F32)).astype(BF16)
     gates = -g_ref[...]
@@ -243,6 +263,12 @@
     def _():
         for copy in across(s, 0):
             copy.start()
+
+    for i, fill in enumerate(fills):
+        if i not in first:
+            fill.wait()
+    for load in loads:
+        load.start()
 
     qf_ref[...] = q_ref[...].astype(F32)
     row = lax.broadcasted_iota(jnp.int32, (extra, rows), 0)
@@ -720,12 +746,26 @@
     hbm = pl.BlockSpec(memory_space=pl.ANY)
     dma = pltpu.SemaphoreType.DMA
     block = (cap, width)
+    smalls = (
+        queries.reshape(tok_dev * heads, hd),
+        keys.reshape(tok_dev, hd),
+        values.reshape(tok_dev, hd),
+        log_gates,
+        documents[None, :],
+        query_gain[None, :],
+        key_gain[None, :],
+        residual,
+        norm_gain[None, :],
+        routes.T,
+        route_weights.T,
+    )
     return pl.pallas_call(
-        functools.partial(layer_kernel, nz, n_tp),
-        out_shape=jax.ShapeDtypeStruct((rows_dev, width), BF16),
-        in_specs=[vmem] * 7 + [hbm] + [vmem] * 4 + [hbm] * 3,
+        functools.partial(entry, nz, n_tp),
+        out_shape=pltpu.MemorySpace.VMEM((rows_dev, width), BF16),
+        in_specs=[hbm] * 15,
         out_specs=vmem,
-        scratch_shapes=[
+        scratch_shapes=[pltpu.VMEM(small.shape, small.dtype) for small in smalls]
+        + [
             pltpu.VMEM(out_weight.shape, BF16),
             pltpu.VMEM((2, width, hidden_dev), BF16),
             pltpu.VMEM((2, width, hidden_dev), BF16),
@@ -780,28 +820,13 @@
             dma((2, nz)),
             dma((nz,)),
             dma((nz,)),
+            dma((len(smalls),)),
         ],
         compiler_params=pltpu.CompilerParams(
             collective_id=0, has_side_effects=True, vmem_limit_bytes=60 * 1024 * 1024
         ),
         name="layer",
-    )(
-        queries.reshape(tok_dev * heads, hd),
-        keys.reshape(tok_dev, hd),
-        values.reshape(tok_dev, hd),
-        log_gates,
-        documents[None, :],
-        query_gain[None, :],
-        key_gain[None, :],
-        out_weight,
-        residual,
-        norm_gain[None, :],
-        routes.T,
-        route_weights.T,
-        w_gate[0],
-        w_up[0],
-        w_down[0],
-    )
+    )(*smalls[:7], out_weight, *smalls[7:], w_gate[0], w_up[0], w_down[0])
 
 
 def solution(mesh):

time: 91 us -> 87.8 us (0.965)
  Pallas kernels: 89.2 us -> 86.8 us
  local copies, waits for them, and re-layouts: 1.67 us -> 0.71 us
    pallas_call x1, Pallas kernels: 89.2 us -> 86.8 us  [local(): pl.pallas_call(functools.partial(entry, nz, n_tp), out_shape=pltpu.Memory...]
    unnamed x1, local copies, waits for them, and re-layouts: 1.67 us -> 0.71 us
where the time goes in v4:
time: 87.8 us; the launch traced here: 87.5 us
  Pallas kernels  86.8 us (99%)
    pallas_call x1, Pallas kernels, local(): pl.pallas_call(functools.partial(entry, nz, n_tp), out_shape=pltpu.Memory...  86.8 us

profile of v4, /device:TPU:24, one launch (start us, length us, event | category | flops | bytes accessed | tf_op | source)
XLA Modules:
  0.0 87.5 jit_solution(10151476384517106366)
XLA Ops:
  0.0 86.8 %layer.1 = bf16[64,2048]{1,0:T(8,128)(2,1)S(1)} custom-call(bf16[1024,128]{1,0:T(8,128)(2,1)} %bitcast.15, bf16[256,128]{1,0:T(8,128)(2,1)} %bitcast.16, bf16[256,128]{1,0:T(8,128)(2,1)} %bitcast.17, f32[4,256]{1,0:T(4,128)} %refs_3_.1, s32[1,256]{1,0:T(1,128)} %bitcast.19, f32[1,128]{1,0:T(1,128)} %bitcast.22, f32[1,128]{1,0:T(1,128)} %bitcast.23, ...), custom_call_target="tpu_custom_call" | custom-call | tf_op jit(solution)/shard_map/layer/pallas_call | solution.py:762
  86.8 0.7 copy.17

commit v5 on v4

--- a/solution.py
+++ b/solution.py
@@ -216,7 +216,7 @@
     for i in first:
         fills[i].wait()
     k_buf[s] = rms_scale(k_ref[...].astype(F32), kg_ref[...]).astype(BF16)
-    v_buf[s, 0:hd, :] = jnp.transpose(v_ref[...].astype(F32)).astype(BF16)
+    v_buf[s, 0:hd, :] = jnp.transpose(v_ref[...])
     gates = -g_ref[...]
     high = gates.astype(BF16).astype(F32)
     middle = (gates - high).astype(BF16).astype(F32)
@@ -349,7 +349,7 @@
         swap.start()
 
     for h in range(heads):
-        att_ref[:, h * hd:(h + 1) * hd] = jnp.transpose(acc_ref[h] * (1.0 / l_ref[h])).astype(BF16)
+        att_ref[:, h * hd:(h + 1) * hd] = jnp.transpose((acc_ref[h] * (1.0 / l_ref[h])).astype(BF16))
 
     def ho_copy(i):
         return remote(

time: 87.8 us -> 87.8 us (level)
  no operation moved by 1% of the time
where the time goes in v5:
time: 87.8 us; the launch traced here: 87.4 us
  Pallas kernels  86.7 us (99%)
    pallas_call x1, Pallas kernels, local(): pl.pallas_call(functools.partial(entry, nz, n_tp), out_shape=pltpu.Memory...  86.7 us

profile of v5, /device:TPU:24, one launch (start us, length us, event | category | flops | bytes accessed | tf_op | source)
XLA Modules:
  0.0 87.4 jit_solution(4125377691423445537)
XLA Ops:
  0.0 86.7 %layer.1 = bf16[64,2048]{1,0:T(8,128)(2,1)S(1)} custom-call(bf16[1024,128]{1,0:T(8,128)(2,1)} %bitcast.15, bf16[256,128]{1,0:T(8,128)(2,1)} %bitcast.16, bf16[256,128]{1,0:T(8,128)(2,1)} %bitcast.17, f32[4,256]{1,0:T(4,128)} %refs_3_.1, s32[1,256]{1,0:T(1,128)} %bitcast.19, f32[1,128]{1,0:T(1,128)} %bitcast.22, f32[1,128]{1,0:T(1,128)} %bitcast.23, ...), custom_call_target="tpu_custom_call" | custom-call | tf_op jit(solution)/shard_map/layer/pallas_call | solution.py:762
  86.7 0.7 copy.17
